TPU v7x, 256 devices: a whole 4x4x8 slice. The times are simulated.
256 devices in a mesh: row: 32 (over z, x), col: 8 (over y, core).
Axes of the slice: x: 4, y: 4, z: 8, core: 2. Of those that a mesh axis runs over, the one named last changes fastest.
Arguments:
- tokens: bfloat16 [2, 32768, 2048], P(None, ('row', 'col')), may hold values from -6 to 6
- norm_gain: float32 [2048], replicated, may hold values from 0.1 to 1.9
- mix_weight: bfloat16 [2048, 1024], replicated, may hold values from -0.125 to 0.125
- gate_weight: bfloat16 [2048, 2048], replicated, may hold values from -0.125 to 0.125
- out_weight: bfloat16 [1024, 2048], replicated, may hold values from -0.1875 to 0.1875
Outputs:
- gated: bfloat16 [2, 32768, 2048], P(None, ('row', 'col'))
All inputs are finite; a program needn't handle non-finite values.
Results may differ from a plain program's by a relative error of at most 0.017.
Values may be sent and summed in bfloat16 or wider, within the bound.
No kernel may reach another device: no remote copies, remote signals or barrier semaphores. Data moves between devices by JAX's collectives and lax.ppermute only.
A program may use at most 128 MiB of HBM per device.

v0:
```python
import math
import jax
import jax.numpy as jnp
from jax import lax
from jax.sharding import Mesh
from jax.sharding import PartitionSpec as P

GROUP_DIM = 128
LEN1 = 128
ROW = ("row_0", "row_1")
ROW_COL = ("row_0", "row_1", "col")


def cut_along(value, dim, peers):
    before, after = (value.shape[:dim], value.shape[dim + 1 :])
    return jnp.moveaxis(value.reshape(*before, peers, -1, *after), dim, 0)


def laid_out(parts, dim):
    lengths = list(parts.shape[1:])
    lengths[dim] *= parts.shape[0]
    return jnp.moveaxis(parts, 0, dim).reshape(lengths)


def exchange_in_order(parts, axes, order):
    inside = parts.shape[1:]
    whole = parts.reshape(*(lax.axis_size(a) for a in axes), *inside)
    for k in order:
        whole = lax.all_to_all(whole, axes[k], k, k, tiled=True)
    return whole.reshape(-1, *inside)


def one_axis_at_a_time(value, axes, order, split_dim, concat_dim):
    parts = cut_along(value, split_dim, lax.axis_size(axes))
    return laid_out(exchange_in_order(parts, axes, order), concat_dim)


def tables(length, factor):
    indices = jnp.arange(length, dtype=jnp.int32)
    products = indices[:, None] * indices[None, :] % length
    angles = products.astype(jnp.float32) * (2.0 * math.pi / length)
    return (jnp.cos(angles) * factor, jnp.sin(angles) * factor)


def length_transform(values, first_span):
    item_count, span_total, column_count = values.shape
    second_span = span_total // first_span
    cos_first, sin_first = tables(first_span, span_total ** (-0.5))
    cos_second, sin_second = tables(second_span, 1.0)
    row_index = jnp.arange(first_span, dtype=jnp.int32)[:, None]
    col_index = jnp.arange(second_span, dtype=jnp.int32)[None, :]
    twist_angle = (row_index * col_index % span_total).astype(jnp.float32) * (
        2.0 * math.pi / span_total
    )
    twist_cos = jnp.cos(twist_angle)[None, :, :, None]
    twist_sin = jnp.sin(twist_angle)[None, :, :, None]
    arranged = values.reshape(item_count, first_span, second_span, column_count)
    part_real = jnp.einsum("ka,sabc->skbc", cos_first, arranged)
    part_imaginary = -jnp.einsum("ka,sabc->skbc", sin_first, arranged)
    turned_real = part_real * twist_cos + part_imaginary * twist_sin
    turned_imaginary = part_imaginary * twist_cos - part_real * twist_sin
    real_part = jnp.einsum("skbc,bm->smkc", turned_real, cos_second) + jnp.einsum(
        "skbc,bm->smkc", turned_imaginary, sin_second
    )
    imaginary = jnp.einsum("skbc,bm->smkc", turned_imaginary, cos_second) - jnp.einsum(
        "skbc,bm->smkc", turned_real, sin_second
    )
    return (
        real_part.reshape(item_count, span_total, column_count),
        imaginary.reshape(item_count, span_total, column_count),
    )


def local(tokens, norm_gain, mix_weight, gate_weight, out_weight):
    widened = tokens.astype(jnp.float32)
    inverse_rms = lax.rsqrt(jnp.mean(widened * widened, axis=-1, keepdims=True) + 1e-06)
    normed = (widened * inverse_rms * norm_gain).astype(jnp.bfloat16)
    mixed_in = jnp.dot(normed, mix_weight, preferred_element_type=jnp.float32).astype(jnp.bfloat16)
    half_dim = GROUP_DIM // 2
    cos_group, sin_group = tables(GROUP_DIM, GROUP_DIM ** (-0.5))
    left_table = cos_group[:, :half_dim]
    right_table = jnp.concatenate(
        [cos_group[:, half_dim : half_dim + 1], sin_group[:, 1:half_dim]], axis=1
    )
    incoming = lax.all_to_all(mixed_in, "col", split_axis=2, concat_axis=1, tiled=True)
    item_count = incoming.shape[0]
    row_count = incoming.shape[1]
    grouped = incoming.astype(jnp.float32).reshape(item_count, row_count, -1, GROUP_DIM)
    left_part = jnp.einsum("srgj,jk->srgk", grouped, left_table)
    right_part = jnp.einsum("srgj,jk->srgk", grouped, right_table)
    spectra = jnp.stack(
        [
            left_part.reshape(item_count, row_count, -1),
            right_part.reshape(item_count, row_count, -1),
        ],
        axis=2,
    )
    gate_value = jax.nn.sigmoid(jnp.dot(normed, gate_weight, preferred_element_type=jnp.float32))
    seq_count, block_rows = (spectra.shape[0], spectra.shape[1])
    pair_width = spectra.shape[3] // lax.axis_size(ROW)
    flat_index = lax.axis_index(ROW) * pair_width + jnp.arange(pair_width, dtype=jnp.int32)
    lone_pair = flat_index % half_dim == 0
    stacked = lax.all_to_all(
        spectra.astype(jnp.bfloat16), ROW, split_axis=3, concat_axis=1, tiled=True
    ).astype(spectra.dtype)
    width_here = stacked.shape[3]
    joined_in = jnp.concatenate([stacked[:, :, 0], stacked[:, :, 1]], axis=2)
    real_part, imaginary = length_transform(joined_in, LEN1)
    sum_pair = real_part[..., :width_here] + imaginary[..., width_here:]
    diff_pair = real_part[..., :width_here] - imaginary[..., width_here:]
    lower_half = jnp.where(lone_pair, real_part[..., :width_here], sum_pair).astype(jnp.bfloat16)
    upper_half = jnp.where(lone_pair, real_part[..., width_here:], diff_pair).astype(jnp.bfloat16)
    both_halves = jnp.stack([lower_half, upper_half], axis=2)
    returned = one_axis_at_a_time(both_halves, ROW, (0, 1), 1, 3)
    lower_half = returned[:, :, 0].reshape(seq_count, block_rows, -1, half_dim)
    upper_half = returned[:, :, 1].reshape(seq_count, block_rows, -1, half_dim)
    spectral = jnp.concatenate(
        [lower_half, upper_half[..., :1], jnp.flip(upper_half[..., 1:], axis=3)], axis=3
    )
    spectral = spectral.reshape(seq_count, block_rows, -1)
    spectral_rows = lax.all_to_all(spectral, "col", split_axis=1, concat_axis=2, tiled=True)
    mapped = jnp.dot(spectral_rows, out_weight, preferred_element_type=jnp.float32)
    return (gate_value * mapped).astype(jnp.bfloat16)


def solution(mesh):
    split = Mesh(mesh.devices.reshape(8, 4, mesh.shape["col"]), ("row_0", "row_1", "col"))
    return jax.shard_map(
        local,
        mesh=split,
        in_specs=(P(None, ROW_COL, None), P(), P(), P(), P()),
        out_specs=P(None, ROW_COL, None),
        check_vma=False,
    )
```

profile of v0, /device:TPU:1, one launch (start us, length us, event | category | flops | bytes accessed | tf_op | source)
XLA Modules:
  0.0 124.7 jit_solution(7634107121673975796)
XLA Ops:
  0.0 1.5 %fusion.24 = f32[2,128]{1,0:T(2,128)S(1)} fusion(bf16[2,128,2048]{2,1,0:T(8,128)(2,1)} %param.5), kind=kLoop, calls=%fused_computation.14 | loop fusion | flops 1572608 | bytes 1049600 | tf_op jit(solution)/shard_map/reduce_sum | solution.py:76
  1.5 3.8 %fusion.30 = bf16[2,128,1024]{2,1,0:T(8,128)(2,1)S(1)} fusion(bf16[2048,1024]{1,0:T(8,128)(2,1)} %param.7, bf16[2,128,2048]{2,1,0:T(8,128)(2,1)} %param.5, f32[2048]{0:T(1024)} %param.6, f32[2,128]{1,0:T(2,128)S(1)} %add_rsqrt_fusion), kind=kOutput, calls=%fused_computation.24 | convolution fusion | flops 1076101120 | bytes 5776384 | tf_op jit(solution)/shard_map/dot_general | solution.py:78
  5.4 1.1 copy.63
  6.5 6.6 %all-to-all-start = ((bf16[2,128,1024]{1,0,2:T(2,128)(2,1)}), bf16[2,128,1024]{1,0,2:T(2,128)(2,1)S(1)}, u32[]{:S(2)}, u32[]{:S(2)}) async-start(bf16[2,128,1024]{1,0,2:T(2,128)(2,1)} %copy.63), calls=%async_computation | async-start | bytes 1048576 | tf_op jit(solution)/shard_map/all_to_all | solution.py:85
  13.1 0.3 broadcast_multiply_fusion
  13.3 0.3 fusion.81
  13.6 8.8 %all-to-all-done = bf16[2,128,1024]{1,0,2:T(2,128)(2,1)S(1)} async-done(((bf16[2,128,1024]{1,0,2:T(2,128)(2,1)}), bf16[2,128,1024]{1,0,2:T(2,128)(2,1)S(1)}, u32[]{:S(2)}, u32[]{:S(2)}) %all-to-all-start) | async-done | bytes 524320 | tf_op jit(solution)/shard_map/all_to_all | solution.py:85
  22.4 0.5 copy.64
  22.9 0.3 fusion.33
  23.2 0.3 fusion.34
  23.6 1.3 %copy.65 = bf16[2,1024,2,64]{1,0,2,3:T(2,128)(2,1)} copy(bf16[2,1024,2,64]{1,3,0,2:T(8,128)(2,1)S(1)} %pad_maximum_fusion.4) | data formatting | bytes 1048576 | tf_op jit(solution)/shard_map/stack | solution.py:91
  24.9 10.5 %all-to-all-start.1 = ((bf16[2,1024,2,64]{1,0,2,3:T(2,128)(2,1)}), bf16[2,1024,2,64]{1,0,2,3:T(2,128)(2,1)S(1)}, u32[]{:S(2)}, u32[]{:S(2)}) async-start(bf16[2,1024,2,64]{1,0,2,3:T(2,128)(2,1)} %copy.65), calls=%async_computation.1 | async-start | bytes 1048576 | tf_op jit(solution)/shard_map/all_to_all | solution.py:103
  35.5 0.5 fusion.71
  36.0 14.9 %all-to-all-done.1 = bf16[2,1024,2,64]{1,0,2,3:T(2,128)(2,1)S(1)} async-done(((bf16[2,1024,2,64]{1,0,2,3:T(2,128)(2,1)}), bf16[2,1024,2,64]{1,0,2,3:T(2,128)(2,1)S(1)}, u32[]{:S(2)}, u32[]{:S(2)}) %all-to-all-start.1) | async-done | bytes 524320 | tf_op jit(solution)/shard_map/all_to_all | solution.py:103
  50.9 0.3 copy.100
  51.2 0.4 reshape.98
  51.6 0.4 fusion.116
  52.0 0.2 concatenate.16
  52.1 0.2 copy.67
  52.3 0.2 concatenate.17
  52.5 0.2 copy.68
  52.7 0.5 fusion.27
  53.2 0.5 convolution_bitcast_fusion
  53.7 1.3 %fusion.48 = f32[256,2,128,4]{2,0,3,1:T(8,128)S(1)} fusion(f32[2,128,256,4]{1,2,3,0:T(8,128)S(1)} %fusion.27, f32[2,128,256,4]{1,2,3,0:T(8,128)S(1)} %convolution_bitcast_fusion, f32[128,256]{0,1:T(8,128)S(1)} %get-tuple-element.9, f32[128,256]{0,1:T(8,128)S(1)} %get-tuple-element.10), kind=kOutput, calls=%fused_computation.52 | convolution fusion | flops 135921664 | bytes 3407872 | tf_op jit(solution)/shard_map/skbc,bm->smkc/dot_general | solution.py:62
  55.0 1.3 %fusion.46 = f32[256,2,128,4]{2,0,3,1:T(8,128)S(1)} fusion(f32[2,128,256,4]{1,2,3,0:T(8,128)S(1)} %convolution_bitcast_fusion, f32[2,128,256,4]{1,2,3,0:T(8,128)S(1)} %fusion.27, f32[128,256]{0,1:T(8,128)S(1)} %get-tuple-element.9, f32[128,256]{0,1:T(8,128)S(1)} %get-tuple-element.10), kind=kOutput, calls=%fused_computation.50 | convolution fusion | flops 135921664 | bytes 3407872 | tf_op jit(solution)/shard_map/skbc,bm->smkc/dot_general | solution.py:65
  56.3 2.3 %fusion.29 = f32[2,256,128,4]{2,1,3,0:T(8,128)} fusion(f32[256,2,128,4]{2,0,3,1:T(8,128)S(1)} %fusion.48, f32[2,128,256,4]{1,2,3,0:T(8,128)S(1)} %convolution_bitcast_fusion, f32[2,128,256,4]{1,2,3,0:T(8,128)S(1)} %fusion.27, f32[128,256]{0,1:T(8,128)S(1)} %get-tuple-element.9, f32[128,256]{0,1:T(8,128)S(1)} %get-tuple-element.10), kind=kOutput, calls=%fused_computation.23 | convolution fusion | flops 136183808 | bytes 4456448 | tf_op jit(solution)/shard_map/skbc,bm->smkc/dot_general | solution.py:62
  58.6 2.7 %reshape.92 = f32[2,32768,4]{1,2,0:T(4,128)} reshape(f32[2,256,128,4]{2,1,3,0:T(8,128)} %fusion.29) | data formatting | bytes 2097152 | tf_op jit(solution)/shard_map/reshape | solution.py:69
  61.3 2.3 %fusion.28 = f32[2,256,128,4]{2,1,3,0:T(8,128)} fusion(f32[256,2,128,4]{2,0,3,1:T(8,128)S(1)} %fusion.46, f32[2,128,256,4]{1,2,3,0:T(8,128)S(1)} %fusion.27, f32[2,128,256,4]{1,2,3,0:T(8,128)S(1)} %convolution_bitcast_fusion, f32[128,256]{0,1:T(8,128)S(1)} %get-tuple-element.9, f32[128,256]{0,1:T(8,128)S(1)} %get-tuple-element.10), kind=kOutput, calls=%fused_computation.21 | convolution fusion | flops 136183808 | bytes 4456448 | tf_op jit(solution)/shard_map/skbc,bm->smkc/dot_general | solution.py:65
  63.5 1.8 %reshape.93 = f32[2,32768,4]{1,2,0:T(4,128)S(1)} reshape(f32[2,256,128,4]{2,1,3,0:T(8,128)} %fusion.28) | data formatting | bytes 2097152 | tf_op jit(solution)/shard_map/reshape | solution.py:70
  65.3 0.8 fusion.37
  66.1 0.2 stack.14
  66.3 0.2 stack.15
  66.5 0.5 copy.75
  67.1 0.5 copy.76
  67.6 17.5 %all_to_all.52 = bf16[8,4,2,1024,2,2]{3,4,5,1,2,0:T(2,128)(2,1)S(1)} all-to-all(bf16[8,4,2,1024,2,2]{3,4,5,1,2,0:T(2,128)(2,1)S(1)} %copy.76), channel_id=1, replica_groups=mesh['row_0'=8,'row_1'=4,'col'=8] {'row_0'}, dimensions={0} | all-to-all | bytes 1048576 | tf_op jit(solution)/shard_map/all_to_all | solution.py:29
  85.1 0.4 copy.77
  85.5 10.9 %all_to_all.53 = bf16[8,4,2,1024,2,2]{3,4,5,0,2,1:T(2,128)(2,1)S(1)} all-to-all(bf16[8,4,2,1024,2,2]{3,4,5,0,2,1:T(2,128)(2,1)S(1)} %copy.77), channel_id=1, replica_groups=mesh['row_0'=8,'row_1'=4,'col'=8] {'row_1'}, dimensions={1} | all-to-all | bytes 1048576 | tf_op jit(solution)/shard_map/all_to_all | solution.py:29
  96.4 0.5 copy.78
  96.9 0.4 copy.79
  97.4 0.6 slice.60
  97.9 0.5 rev.4
  98.5 1.5 %pad_maximum_fusion.1 = bf16[2,1024,1,128]{1,2,3,0:T(2,128)(2,1)S(1)} fusion(bf16[2,1024,1,63]{1,2,3,0:T(2,128)(2,1)S(1)} %rev.4, bf16[2,1024,1,1]{1,2,3,0:T(2,128)(2,1)S(1)} %slice.59, bf16[2,1024,1,64]{1,2,3,0:T(2,128)(2,1)S(1)} %bitcast.112), kind=kLoop, calls=%fused_computation.30 | loop fusion | flops 524288 | bytes 1048576 | tf_op jit(solution)/shard_map/concatenate | solution.py:117
  100.0 0.9 copy.80
  100.9 1.3 %copy.81 = bf16[2,1024,128]{2,0,1:T(2,128)(2,1)} copy(bf16[2,1024,128]{2,1,0:T(8,128)(2,1)S(1)} %bitcast.113) | data formatting | bytes 1048576 | tf_op jit(solution)/shard_map/reshape | solution.py:120
  102.2 8.5 %all-to-all-start.4 = ((bf16[2,1024,128]{2,0,1:T(2,128)(2,1)}), bf16[2,1024,128]{2,0,1:T(2,128)(2,1)S(1)}, u32[]{:S(2)}, u32[]{:S(2)}) async-start(bf16[2,1024,128]{2,0,1:T(2,128)(2,1)} %copy.81), calls=%async_computation.4 | async-start | bytes 1048576 | tf_op jit(solution)/shard_map/all_to_all | solution.py:121
  110.8 6.2 %fusion.21 = f32[2,128,2048]{2,1,0:T(8,128)S(1)} fusion(bf16[2048,2048]{1,0:T(8,128)(2,1)} %param.8, bf16[2,128,2048]{2,1,0:T(8,128)(2,1)} %param.5, f32[2048]{0:T(1024)S(1)} %copy-done.1, f32[2,128]{1,0:T(2,128)S(1)} %add_rsqrt_fusion), kind=kOutput, calls=%fused_computation.13 | convolution fusion | flops 2151153664 | bytes 11543552 | tf_op jit(solution)/shard_map/dot_general | solution.py:98
  117.0 3.2 %all-to-all-done.4 = bf16[2,1024,128]{2,0,1:T(2,128)(2,1)S(1)} async-done(((bf16[2,1024,128]{2,0,1:T(2,128)(2,1)}), bf16[2,1024,128]{2,0,1:T(2,128)(2,1)S(1)}, u32[]{:S(2)}, u32[]{:S(2)}) %all-to-all-start.4) | async-done | bytes 524320 | tf_op jit(solution)/shard_map/all_to_all | solution.py:121
  120.2 4.5 %fusion.18 = bf16[2,128,2048]{2,1,0:T(8,128)(2,1)} fusion(f32[2,128,2048]{2,1,0:T(8,128)S(1)} %fusion.21, bf16[1024,2048]{1,0:T(8,128)(2,1)} %param.9, bf16[2,8,16,8,128]{4,3,2,1,0:T(8,128)(2,1)S(1)} %bitcast.119), kind=kOutput, calls=%fused_computation.12 | convolution fusion | flops 1074790400 | bytes 7864320 | tf_op jit(solution)/shard_map/dot_general | solution.py:122
  (12 shorter events, 0.2 us)
Async XLA Ops:
  6.5 16.0 %all-to-all-start = ((bf16[2,128,1024]{1,0,2:T(2,128)(2,1)}), bf16[2,128,1024]{1,0,2:T(2,128)(2,1)S(1)}, u32[]{:S(2)}, u32[]{:S(2)}) async-start(bf16[2,128,1024]{1,0,2:T(2,128)(2,1)} %copy.63), calls=%async_computation | async-start | bytes 1048576 | tf_op jit(solution)/shard_map/all_to_all | solution.py:85
  24.9 26.0 %all-to-all-start.1 = ((bf16[2,1024,2,64]{1,0,2,3:T(2,128)(2,1)}), bf16[2,1024,2,64]{1,0,2,3:T(2,128)(2,1)S(1)}, u32[]{:S(2)}, u32[]{:S(2)}) async-start(bf16[2,1024,2,64]{1,0,2,3:T(2,128)(2,1)} %copy.65), calls=%async_computation.1 | async-start | bytes 1048576 | tf_op jit(solution)/shard_map/all_to_all | solution.py:103
  63.5 1.8 %copy-start = (f32[2,32768,4]{1,2,0:T(4,128)S(1)}, f32[2,32768,4]{1,2,0:T(4,128)}, u32[]{:S(2)}) copy-start(f32[2,32768,4]{1,2,0:T(4,128)} %reshape.92) | copy-start | bytes 3145732
  100.0 10.8 %copy-start.1 = (f32[2048]{0:T(1024)S(1)}, f32[2048]{0:T(1024)}, u32[]{:S(2)}) copy-start(f32[2048]{0:T(1024)} %param.6) | copy-start | bytes 24580
  102.2 17.9 %all-to-all-start.4 = ((bf16[2,1024,128]{2,0,1:T(2,128)(2,1)}), bf16[2,1024,128]{2,0,1:T(2,128)(2,1)S(1)}, u32[]{:S(2)}, u32[]{:S(2)}) async-start(bf16[2,1024,128]{2,0,1:T(2,128)(2,1)} %copy.81), calls=%async_computation.4 | async-start | bytes 1048576 | tf_op jit(solution)/shard_map/all_to_all | solution.py:121
where the time goes:
time: 125 us
  blocking collectives  28.4 us (23%)
  waiting for transfers between devices  26.9 us (22%)
  starting transfers between devices  25.7 us (21%)
  matrix products  23.3 us (19%)
  local copies, waits for them, and re-layouts  15.2 us (12%)
  other arithmetic  4.97 us (4%)
    all_to_all x2, blocking collectives, exchange_in_order(): whole = lax.all_to_all(whole, axes[k], k, k, tiled=True)  28.4 us
    all_to_all x1, waiting for transfers between devices, local(): lax.all_to_all(spectra.astype(jnp.bfloat16), ROW, split_axis=3, concat_ax...  14.9 us
    all_to_all x1, starting transfers between devices, local(): lax.all_to_all(spectra.astype(jnp.bfloat16), ROW, split_axis=3, concat_ax...  10.5 us
    all_to_all x1, waiting for transfers between devices, local(): lax.all_to_all(mixed_in, 'col', split_axis=2, concat_axis=1, tiled=True)  8.82 us
    all_to_all x1, starting transfers between devices, local(): lax.all_to_all(spectral, 'col', split_axis=1, concat_axis=2, tiled=True)  8.54 us
    all_to_all x1, starting transfers between devices, local(): lax.all_to_all(mixed_in, 'col', split_axis=2, concat_axis=1, tiled=True)  6.6 us
    dot_general x1, matrix products, local(): jnp.dot(normed, gate_weight, preferred_element_type=jnp.float32)  6.2 us
    dot_general x1, matrix products, local(): jnp.dot(spectral_rows, out_weight, preferred_element_type=jnp.float32)  4.48 us
  transfers between devices with their start and end apart: 3, of which 3 were waited for; matrix products, arithmetic and copies ran while one was open for 6% of the time, Pallas kernels for 0%

commit v1 on v0

--- a/solution.py
+++ b/solution.py
@@ -82,7 +82,10 @@
     right_table = jnp.concatenate(
         [cos_group[:, half_dim : half_dim + 1], sin_group[:, 1:half_dim]], axis=1
     )
-    incoming = lax.all_to_all(mixed_in, "col", split_axis=2, concat_axis=1, tiled=True)
+    incoming = jnp.concatenate(
+        lax.all_to_all(jnp.stack(jnp.split(mixed_in, lax.axis_size("col"), axis=2)), "col", 0, 0),
+        axis=1,
+    )
     item_count = incoming.shape[0]
     row_count = incoming.shape[1]
     grouped = incoming.astype(jnp.float32).reshape(item_count, row_count, -1, GROUP_DIM)

time: 125 us -> 129 us (1.032)
  local copies, waits for them, and re-layouts: 15.2 us -> 18.9 us
    unnamed x4 -> x11, local copies, waits for them, and re-layouts: 0.01 us -> 4.54 us
where the time goes in v1:
time: 129 us; the launch traced here: 128 us
  blocking collectives  28.4 us (22%)
  waiting for transfers between devices  26.9 us (21%)
  starting transfers between devices  25.7 us (20%)
  matrix products  23.3 us (18%)
  local copies, waits for them, and re-layouts  18.9 us (15%)
  other arithmetic  4.97 us (4%)
    all_to_all x2, blocking collectives, exchange_in_order(): whole = lax.all_to_all(whole, axes[k], k, k, tiled=True)  28.4 us
    all_to_all x1, waiting for transfers between devices, local(): lax.all_to_all(spectra.astype(jnp.bfloat16), ROW, split_axis=3, concat_ax...  14.9 us
    all_to_all x1, starting transfers between devices, local(): lax.all_to_all(spectra.astype(jnp.bfloat16), ROW, split_axis=3, concat_ax...  10.6 us
    all_to_all x1, waiting for transfers between devices, local(): lax.all_to_all(jnp.stack(jnp.split(mixed_in, lax.axis_size('col'), axis=2...  8.82 us
    all_to_all x1, starting transfers between devices, local(): lax.all_to_all(spectral, 'col', split_axis=1, concat_axis=2, tiled=True)  8.54 us
    all_to_all x1, starting transfers between devices, local(): lax.all_to_all(jnp.stack(jnp.split(mixed_in, lax.axis_size('col'), axis=2...  6.6 us
    dot_general x1, matrix products, local(): jnp.dot(normed, gate_weight, preferred_element_type=jnp.float32)  6.2 us
    unnamed x11, local copies, waits for them, and re-layouts  4.54 us
  transfers between devices with their start and end apart: 3, of which 3 were waited for; matrix products, arithmetic and copies ran while one was open for 6% of the time, Pallas kernels for 0%

profile of v1, /device:TPU:1, one launch (start us, length us, event | category | flops | bytes accessed | tf_op | source)
XLA Modules:
  0.0 128.4 jit_solution(14056710694698260826)
XLA Ops:
  0.0 1.5 %fusion.24 = f32[2,128]{1,0:T(2,128)S(1)} fusion(bf16[2,128,2048]{2,1,0:T(8,128)(2,1)} %param.5), kind=kLoop, calls=%fused_computation.14 | loop fusion | flops 1572608 | bytes 1049600 | tf_op jit(solution)/shard_map/reduce_sum | solution.py:76
  1.5 3.8 %fusion.30 = bf16[2,128,1024]{2,1,0:T(8,128)(2,1)S(1)} fusion(bf16[2048,1024]{1,0:T(8,128)(2,1)} %param.7, bf16[2,128,2048]{2,1,0:T(8,128)(2,1)} %param.5, f32[2048]{0:T(1024)} %param.6, f32[2,128]{1,0:T(2,128)S(1)} %add_rsqrt_fusion), kind=kOutput, calls=%fused_computation.24 | convolution fusion | flops 1076101120 | bytes 5776384 | tf_op jit(solution)/shard_map/dot_general | solution.py:78
  5.4 0.6 fusion.75
  6.0 0.6 fusion.74
  6.6 0.6 fusion.73
  7.3 0.6 fusion.72
  7.9 0.6 fusion.71
  8.6 0.6 fusion.70
  9.2 0.6 fusion.69
  9.9 0.6 fusion.68
  10.5 6.6 %all-to-all-start = ((bf16[8,2,128,128]{3,2,1,0:T(8,128)(2,1)}), bf16[8,2,128,128]{3,2,1,0:T(8,128)(2,1)S(1)}, u32[]{:S(2)}, u32[]{:S(2)}) async-start(bf16[8,2,128,128]{3,2,1,0:T(8,128)(2,1)} %fusion.68), calls=%async_computation | async-start | bytes 1048576 | tf_op jit(solution)/shard_map/all_to_all | solution.py:86
  17.1 0.3 broadcast_multiply_fusion
  17.4 0.3 fusion.89
  17.7 8.8 %all-to-all-done = bf16[8,2,128,128]{3,2,1,0:T(8,128)(2,1)S(1)} async-done(((bf16[8,2,128,128]{3,2,1,0:T(8,128)(2,1)}), bf16[8,2,128,128]{3,2,1,0:T(8,128)(2,1)S(1)}, u32[]{:S(2)}, u32[]{:S(2)}) %all-to-all-start) | async-done | bytes 524320 | tf_op jit(solution)/shard_map/all_to_all | solution.py:86
  26.6 0.3 fusion.33
  26.9 0.3 fusion.34
  27.2 1.3 %copy.61 = bf16[2,1024,2,64]{1,0,2,3:T(2,128)(2,1)} copy(bf16[2,1024,2,64]{1,3,0,2:T(8,128)(2,1)S(1)} %pad_maximum_fusion.4) | data formatting | bytes 1048576 | tf_op jit(solution)/shard_map/stack | solution.py:94
  28.6 10.6 %all-to-all-start.1 = ((bf16[2,1024,2,64]{1,0,2,3:T(2,128)(2,1)}), bf16[2,1024,2,64]{1,0,2,3:T(2,128)(2,1)S(1)}, u32[]{:S(2)}, u32[]{:S(2)}) async-start(bf16[2,1024,2,64]{1,0,2,3:T(2,128)(2,1)} %copy.61), calls=%async_computation.1 | async-start | bytes 1048576 | tf_op jit(solution)/shard_map/all_to_all | solution.py:106
  39.1 0.5 fusion.79
  39.7 14.9 %all-to-all-done.1 = bf16[2,1024,2,64]{1,0,2,3:T(2,128)(2,1)S(1)} async-done(((bf16[2,1024,2,64]{1,0,2,3:T(2,128)(2,1)}), bf16[2,1024,2,64]{1,0,2,3:T(2,128)(2,1)S(1)}, u32[]{:S(2)}, u32[]{:S(2)}) %all-to-all-start.1) | async-done | bytes 524320 | tf_op jit(solution)/shard_map/all_to_all | solution.py:106
  54.6 0.3 copy.96
  54.9 0.4 reshape.103
  55.2 0.4 fusion.124
  56.3 0.5 fusion.27
  56.9 0.5 convolution_bitcast_fusion
  57.4 1.3 %fusion.48 = f32[256,2,128,4]{2,0,3,1:T(8,128)S(1)} fusion(f32[2,128,256,4]{1,2,3,0:T(8,128)S(1)} %fusion.27, f32[2,128,256,4]{1,2,3,0:T(8,128)S(1)} %convolution_bitcast_fusion, f32[128,256]{0,1:T(8,128)S(1)} %get-tuple-element.9, f32[128,256]{0,1:T(8,128)S(1)} %get-tuple-element.10), kind=kOutput, calls=%fused_computation.52 | convolution fusion | flops 135921664 | bytes 3407872 | tf_op jit(solution)/shard_map/skbc,bm->smkc/dot_general | solution.py:62
  58.7 1.3 %fusion.46 = f32[256,2,128,4]{2,0,3,1:T(8,128)S(1)} fusion(f32[2,128,256,4]{1,2,3,0:T(8,128)S(1)} %convolution_bitcast_fusion, f32[2,128,256,4]{1,2,3,0:T(8,128)S(1)} %fusion.27, f32[128,256]{0,1:T(8,128)S(1)} %get-tuple-element.9, f32[128,256]{0,1:T(8,128)S(1)} %get-tuple-element.10), kind=kOutput, calls=%fused_computation.50 | convolution fusion | flops 135921664 | bytes 3407872 | tf_op jit(solution)/shard_map/skbc,bm->smkc/dot_general | solution.py:65
  60.0 2.3 %fusion.29 = f32[2,256,128,4]{2,1,3,0:T(8,128)} fusion(f32[256,2,128,4]{2,0,3,1:T(8,128)S(1)} %fusion.48, f32[2,128,256,4]{1,2,3,0:T(8,128)S(1)} %convolution_bitcast_fusion, f32[2,128,256,4]{1,2,3,0:T(8,128)S(1)} %fusion.27, f32[128,256]{0,1:T(8,128)S(1)} %get-tuple-element.9, f32[128,256]{0,1:T(8,128)S(1)} %get-tuple-element.10), kind=kOutput, calls=%fused_computation.23 | convolution fusion | flops 136183808 | bytes 4456448 | tf_op jit(solution)/shard_map/skbc,bm->smkc/dot_general | solution.py:62
  62.3 2.7 %reshape.97 = f32[2,32768,4]{1,2,0:T(4,128)} reshape(f32[2,256,128,4]{2,1,3,0:T(8,128)} %fusion.29) | data formatting | bytes 2097152 | tf_op jit(solution)/shard_map/reshape | solution.py:69
  64.9 2.3 %fusion.28 = f32[2,256,128,4]{2,1,3,0:T(8,128)} fusion(f32[256,2,128,4]{2,0,3,1:T(8,128)S(1)} %fusion.46, f32[2,128,256,4]{1,2,3,0:T(8,128)S(1)} %fusion.27, f32[2,128,256,4]{1,2,3,0:T(8,128)S(1)} %convolution_bitcast_fusion, f32[128,256]{0,1:T(8,128)S(1)} %get-tuple-element.9, f32[128,256]{0,1:T(8,128)S(1)} %get-tuple-element.10), kind=kOutput, calls=%fused_computation.21 | convolution fusion | flops 136183808 | bytes 4456448 | tf_op jit(solution)/shard_map/skbc,bm->smkc/dot_general | solution.py:65
  67.2 1.8 %reshape.98 = f32[2,32768,4]{1,2,0:T(4,128)S(1)} reshape(f32[2,256,128,4]{2,1,3,0:T(8,128)} %fusion.28) | data formatting | bytes 2097152 | tf_op jit(solution)/shard_map/reshape | solution.py:70
  69.0 0.8 fusion.37
  70.2 0.5 copy.71
  70.7 0.5 copy.72
  71.3 17.4 %all_to_all.42 = bf16[8,4,2,1024,2,2]{3,4,5,1,2,0:T(2,128)(2,1)S(1)} all-to-all(bf16[8,4,2,1024,2,2]{3,4,5,1,2,0:T(2,128)(2,1)S(1)} %copy.72), channel_id=1, replica_groups=mesh['row_0'=8,'row_1'=4,'col'=8] {'row_0'}, dimensions={0} | all-to-all | bytes 1048576 | tf_op jit(solution)/shard_map/all_to_all | solution.py:29
  88.7 0.4 copy.73
  89.1 10.9 %all_to_all.43 = bf16[8,4,2,1024,2,2]{3,4,5,0,2,1:T(2,128)(2,1)S(1)} all-to-all(bf16[8,4,2,1024,2,2]{3,4,5,0,2,1:T(2,128)(2,1)S(1)} %copy.73), channel_id=1, replica_groups=mesh['row_0'=8,'row_1'=4,'col'=8] {'row_1'}, dimensions={1} | all-to-all | bytes 1048576 | tf_op jit(solution)/shard_map/all_to_all | solution.py:29
  100.0 0.5 copy.74
  100.6 0.4 copy.75
  101.0 0.6 slice.60
  101.6 0.5 rev.4
  102.1 1.5 %pad_maximum_fusion.1 = bf16[2,1024,1,128]{1,2,3,0:T(2,128)(2,1)S(1)} fusion(bf16[2,1024,1,63]{1,2,3,0:T(2,128)(2,1)S(1)} %rev.4, bf16[2,1024,1,1]{1,2,3,0:T(2,128)(2,1)S(1)} %slice.59, bf16[2,1024,1,64]{1,2,3,0:T(2,128)(2,1)S(1)} %bitcast.142), kind=kLoop, calls=%fused_computation.30 | loop fusion | flops 524288 | bytes 1048576 | tf_op jit(solution)/shard_map/concatenate | solution.py:120
  103.7 0.9 copy.76
  104.5 1.3 %copy.77 = bf16[2,1024,128]{2,0,1:T(2,128)(2,1)} copy(bf16[2,1024,128]{2,1,0:T(8,128)(2,1)S(1)} %bitcast.143) | data formatting | bytes 1048576 | tf_op jit(solution)/shard_map/reshape | solution.py:123
  105.9 8.5 %all-to-all-start.4 = ((bf16[2,1024,128]{2,0,1:T(2,128)(2,1)}), bf16[2,1024,128]{2,0,1:T(2,128)(2,1)S(1)}, u32[]{:S(2)}, u32[]{:S(2)}) async-start(bf16[2,1024,128]{2,0,1:T(2,128)(2,1)} %copy.77), calls=%async_computation.4 | async-start | bytes 1048576 | tf_op jit(solution)/shard_map/all_to_all | solution.py:124
  114.4 6.2 %fusion.21 = f32[2,128,2048]{2,1,0:T(8,128)S(1)} fusion(bf16[2048,2048]{1,0:T(8,128)(2,1)} %param.8, bf16[2,128,2048]{2,1,0:T(8,128)(2,1)} %param.5, f32[2048]{0:T(1024)S(1)} %copy-done.1, f32[2,128]{1,0:T(2,128)S(1)} %add_rsqrt_fusion), kind=kOutput, calls=%fused_computation.13 | convolution fusion | flops 2151153664 | bytes 11543552 | tf_op jit(solution)/shard_map/dot_general | solution.py:101
  120.6 3.2 %all-to-all-done.4 = bf16[2,1024,128]{2,0,1:T(2,128)(2,1)S(1)} async-done(((bf16[2,1024,128]{2,0,1:T(2,128)(2,1)}), bf16[2,1024,128]{2,0,1:T(2,128)(2,1)S(1)}, u32[]{:S(2)}, u32[]{:S(2)}) %all-to-all-start.4) | async-done | bytes 524320 | tf_op jit(solution)/shard_map/all_to_all | solution.py:124
  123.9 4.5 %fusion.18 = bf16[2,128,2048]{2,1,0:T(8,128)(2,1)} fusion(f32[2,128,2048]{2,1,0:T(8,128)S(1)} %fusion.21, bf16[1024,2048]{1,0:T(8,128)(2,1)} %param.9, bf16[2,8,16,8,128]{4,3,2,1,0:T(8,128)(2,1)S(1)} %bitcast.149), kind=kOutput, calls=%fused_computation.12 | convolution fusion | flops 1074790400 | bytes 7864320 | tf_op jit(solution)/shard_map/dot_general | solution.py:125
  (19 shorter events, 1.3 us)
Async XLA Ops:
  10.5 16.0 %all-to-all-start = ((bf16[8,2,128,128]{3,2,1,0:T(8,128)(2,1)}), bf16[8,2,128,128]{3,2,1,0:T(8,128)(2,1)S(1)}, u32[]{:S(2)}, u32[]{:S(2)}) async-start(bf16[8,2,128,128]{3,2,1,0:T(8,128)(2,1)} %fusion.68), calls=%async_computation | async-start | bytes 1048576 | tf_op jit(solution)/shard_map/all_to_all | solution.py:86
  28.6 26.0 %all-to-all-start.1 = ((bf16[2,1024,2,64]{1,0,2,3:T(2,128)(2,1)}), bf16[2,1024,2,64]{1,0,2,3:T(2,128)(2,1)S(1)}, u32[]{:S(2)}, u32[]{:S(2)}) async-start(bf16[2,1024,2,64]{1,0,2,3:T(2,128)(2,1)} %copy.61), calls=%async_computation.1 | async-start | bytes 1048576 | tf_op jit(solution)/shard_map/all_to_all | solution.py:106
  67.2 1.8 %copy-start = (f32[2,32768,4]{1,2,0:T(4,128)S(1)}, f32[2,32768,4]{1,2,0:T(4,128)}, u32[]{:S(2)}) copy-start(f32[2,32768,4]{1,2,0:T(4,128)} %reshape.97) | copy-start | bytes 3145732
  103.7 10.8 %copy-start.1 = (f32[2048]{0:T(1024)S(1)}, f32[2048]{0:T(1024)}, u32[]{:S(2)}) copy-start(f32[2048]{0:T(1024)} %param.6) | copy-start | bytes 24580
  105.9 17.9 %all-to-all-start.4 = ((bf16[2,1024,128]{2,0,1:T(2,128)(2,1)}), bf16[2,1024,128]{2,0,1:T(2,128)(2,1)S(1)}, u32[]{:S(2)}, u32[]{:S(2)}) async-start(bf16[2,1024,128]{2,0,1:T(2,128)(2,1)} %copy.77), calls=%async_computation.4 | async-start | bytes 1048576 | tf_op jit(solution)/shard_map/all_to_all | solution.py:124
